TPU v7x, 512 devices: a 8x2x16 block of a 8x16x16 slice. The times are simulated.
512 devices in a mesh: grp: 2 (over y), kv: 16 (over z), tp: 16 (over x, core).
Axes of the slice: x: 8, y: 2, z: 16, core: 2. Of those that a mesh axis runs over, the one named last changes fastest.
The devices are a block of a 8x16x16 slice.
Arguments:
- stream_in: bfloat16 [384, 4096], P(('grp', 'tp'), 'kv'), parts along dimension 0, may hold values from -40 to 40
- positions: int32 [384], P(('grp', 'kv')), parts along dimension 0, may hold values from 1024 to 32767
- ret_state: float32 [384, 16, 128, 128], P(('grp', 'kv'), 'tp'), parts along dimension 0, may hold values from -0.6 to 0.6
- first_gain: float32 [4096], P('kv'), may hold values from 0.1 to 1.9
- first_gate: bfloat16 [4096, 11008], P('kv', 'tp'), may hold values from -0.09375 to 0.09375
- first_up: bfloat16 [4096, 11008], P('kv', 'tp'), may hold values from -0.09375 to 0.09375
- first_down: bfloat16 [11008, 4096], P('tp', 'kv'), may hold values from -0.1875 to 0.1875
- mix_gain: float32 [4096], P('kv'), may hold values from 0.1 to 1.9
- w_query: bfloat16 [4096, 2048], P('kv', 'tp'), may hold values from -0.09375 to 0.09375
- w_key: bfloat16 [4096, 2048], P('kv', 'tp'), may hold values from -0.09375 to 0.09375
- w_value: bfloat16 [4096, 2048], P('kv', 'tp'), may hold values from -0.09375 to 0.09375
- w_outgate: bfloat16 [4096, 2048], P('kv', 'tp'), may hold values from -0.09375 to 0.09375
- w_out: bfloat16 [2048, 4096], P('tp', 'kv'), may hold values from -0.21875 to 0.21875
- head_gain: float32 [2048], P('tp'), may hold values from 0.1 to 1.9
- second_gain: float32 [4096], P('kv'), may hold values from 0.1 to 1.9
- second_gate: bfloat16 [4096, 11008], P('kv', 'tp'), may hold values from -0.09375 to 0.09375
- second_up: bfloat16 [4096, 11008], P('kv', 'tp'), may hold values from -0.09375 to 0.09375
- second_down: bfloat16 [11008, 4096], P('tp', 'kv'), may hold values from -0.1875 to 0.1875
Outputs:
- stream_out: bfloat16 [384, 4096], P(('grp', 'tp'), 'kv'), parts along dimension 0
- new_state: float32 [384, 16, 128, 128], P(('grp', 'kv'), 'tp'), parts along dimension 0
There are 2 independent parts, one for each index of `grp`. A program takes and returns all parts, laid end to end along the dimension named above; an argument that names none is the same for every part. Nothing has to cross between parts.
All inputs are finite; a program needn't handle non-finite values.
Results may differ from a plain program's by a relative error of at most 0.03.
Values may be sent and summed in bfloat16 or wider, within the bound.
No kernel may reach another device: no remote copies, remote signals or barrier semaphores. Data moves between devices by JAX's collectives and lax.ppermute only.
A program may use at most 64 MiB of HBM per device.

v0:
```python
import jax
import jax.numpy as jnp
from jax import lax
from jax.sharding import PartitionSpec as P

D = 4096
EPS_NORM = 1e-06
EPS_GROUP = 1e-05


def in_blocks(x, dim, length):
    lengths = x.shape
    parts = x.reshape(*lengths[:dim], length, lengths[dim] // length, *lengths[dim + 1 :])
    return jnp.moveaxis(parts, dim, 0)


def sent_and_summed(x, axis, dim):
    parts = in_blocks(x, dim, lax.axis_size(axis))
    arrived = lax.all_to_all(parts, axis, split_axis=0, concat_axis=0, tiled=True)
    return arrived.astype(jnp.float32).sum(axis=0)


def sent_together(arrays, axis, dim, along):
    columns = [a.reshape(*a.shape[:along], -1) for a in arrays]
    both = jnp.concatenate(columns, axis=along)
    filled, at, done = (sent_and_summed(both, axis, dim), 0, [])
    for a, column in zip(arrays, columns):
        section = filled[..., at : at + column.shape[along]]
        done.append(section.reshape(*section.shape[:along], *a.shape[along:]))
        at += column.shape[along]
    return tuple(done)


def from_everyone(x, axis):
    length = lax.axis_size(axis)
    return lax.all_to_all(jnp.broadcast_to(x[None], (length, *x.shape)), axis, 0, 0, tiled=True)


def joined_along(parts, dim):
    parts = jnp.moveaxis(parts, 0, dim)
    lengths = parts.shape
    return parts.reshape(*lengths[:dim], lengths[dim] * lengths[dim + 1], *lengths[dim + 2 :])


def collect(x, axis, dim):
    parts = from_everyone(x, axis)
    return joined_along(parts, dim)


def widen_rows(stream_rows):
    return lax.all_gather(stream_rows, "tp", axis=0, tiled=True)


def prepare(stream, norm_gain):
    widened = stream.astype(jnp.float32)
    squares = jnp.sum(widened * widened, axis=1)
    scaled = (widened * norm_gain).astype(jnp.bfloat16)
    return (squares, scaled)


def feed_forward(stream, norm_gain, w_gate, w_up):
    squares, scaled = prepare(stream, norm_gain)
    gate_part = jnp.dot(scaled, w_gate, preferred_element_type=jnp.float32)
    up_part = jnp.dot(scaled, w_up, preferred_element_type=jnp.float32)
    gate_part, up_part, squares = sent_together(
        (
            gate_part.astype(jnp.bfloat16),
            up_part.astype(jnp.bfloat16),
            squares.astype(jnp.bfloat16),
        ),
        "kv",
        0,
        1,
    )
    factor = lax.rsqrt(squares / D + EPS_NORM)[:, None]
    own_hidden = (jax.nn.silu(factor * gate_part) * (factor * up_part)).astype(jnp.bfloat16)
    return collect(own_hidden, "kv", 0)


def advance(stream, inputs_back, weight_back, factor_branch):
    row_count = stream.shape[0] // lax.axis_size("tp")
    row_share = sent_and_summed(
        jnp.dot(inputs_back, weight_back, preferred_element_type=jnp.float32).astype(jnp.bfloat16),
        "tp",
        0,
    )
    own_rows = lax.dynamic_slice_in_dim(stream, lax.axis_index("tp") * row_count, row_count, 0)
    return (own_rows.astype(jnp.float32) + factor_branch * row_share).astype(jnp.bfloat16)


def rotate(values_in, cosine, sine_part):
    half_dim = values_in.shape[-1] // 2
    lower_half = values_in[..., :half_dim]
    upper_half = values_in[..., half_dim:]
    return jnp.concatenate(
        [
            lower_half * cosine - upper_half * sine_part,
            lower_half * sine_part + upper_half * cosine,
        ],
        axis=-1,
    )


def retention(
    stream, norm_gain, w_query, w_key, w_value, w_outgate, head_gain, state_old, positions
):
    squares, scaled = prepare(stream, norm_gain)
    query_part = jnp.dot(scaled, w_query, preferred_element_type=jnp.float32)
    key_part = jnp.dot(scaled, w_key, preferred_element_type=jnp.float32)
    value_part = jnp.dot(scaled, w_value, preferred_element_type=jnp.float32)
    gate_part = jnp.dot(scaled, w_outgate, preferred_element_type=jnp.float32)
    query_part, key_part, value_part, gate_part, squares = sent_together(
        (
            query_part.astype(jnp.bfloat16),
            key_part.astype(jnp.bfloat16),
            value_part.astype(jnp.bfloat16),
            gate_part.astype(jnp.bfloat16),
            squares.astype(jnp.bfloat16),
        ),
        "kv",
        0,
        1,
    )
    factor = lax.rsqrt(squares / D + EPS_NORM)[:, None]
    sequences = state_old.shape[0]
    head_count = state_old.shape[1]
    width_head = state_old.shape[2]
    shape_heads = (sequences, head_count, width_head)
    queries = (factor * query_part).reshape(shape_heads)
    key_vec = (factor * key_part).reshape(shape_heads)
    values_new = (factor * value_part).reshape(shape_heads)
    gate_pre = (factor * gate_part).reshape(shape_heads)
    half_dim = width_head // 2
    inverse = 10000.0 ** (-jnp.arange(half_dim, dtype=jnp.float32) / half_dim)
    angles = positions.astype(jnp.float32)[:, None] * inverse[None, :]
    cosine = jnp.cos(angles)[:, None, :]
    sine_part = jnp.sin(angles)[:, None, :]
    queries = rotate(queries, cosine, sine_part)
    key_vec = rotate(key_vec, cosine, sine_part) * width_head ** (-0.5)
    head_ids = (lax.axis_index("tp") * head_count + jnp.arange(head_count)).astype(jnp.float32)
    decays = jnp.exp(jnp.log1p(-(2.0 ** (-5.0 - head_ids))))
    carried = jnp.einsum("shd,shde->she", queries, state_old, precision=lax.Precision.HIGHEST)
    within = jnp.sum(queries * key_vec, axis=-1, keepdims=True)
    mixture = decays[None, :, None] * carried + within * values_new
    new_state = (
        decays[None, :, None, None] * state_old + key_vec[..., :, None] * values_new[..., None, :]
    )
    average = jnp.mean(mixture, axis=-1, keepdims=True)
    centered = mixture - average
    variance = jnp.mean(centered * centered, axis=-1, keepdims=True)
    normed = centered * lax.rsqrt(variance + EPS_GROUP) * head_gain.reshape(head_count, width_head)
    ret_out = (
        (jax.nn.silu(gate_pre) * normed)
        .astype(jnp.bfloat16)
        .reshape(sequences, head_count * width_head)
    )
    return (collect(ret_out, "kv", 0), new_state)


def per_device(
    stream_in,
    positions,
    ret_state,
    first_gain,
    first_gate,
    first_up,
    first_down,
    mix_gain,
    w_query,
    w_key,
    w_value,
    w_outgate,
    w_out,
    head_gain,
    second_gain,
    second_gate,
    second_up,
    second_down,
):
    stream = widen_rows(stream_in)
    hidden = feed_forward(stream, first_gain, first_gate, first_up)
    stream = advance(stream, hidden, first_down, 0.5)
    stream = widen_rows(stream)
    ret_out, new_state = retention(
        stream, mix_gain, w_query, w_key, w_value, w_outgate, head_gain, ret_state, positions
    )
    stream = advance(stream, ret_out, w_out, 1.0)
    stream = widen_rows(stream)
    hidden = feed_forward(stream, second_gain, second_gate, second_up)
    stream = advance(stream, hidden, second_down, 0.5)
    return (stream, new_state)


def solution(mesh):
    in_specs = (
        P(("grp", "tp"), "kv"),
        P(("grp", "kv")),
        P(("grp", "kv"), "tp", None, None),
        P("kv"),
        P("kv", "tp"),
        P("kv", "tp"),
        P("tp", "kv"),
        P("kv"),
        P("kv", "tp"),
        P("kv", "tp"),
        P("kv", "tp"),
        P("kv", "tp"),
        P("tp", "kv"),
        P("tp"),
        P("kv"),
        P("kv", "tp"),
        P("kv", "tp"),
        P("tp", "kv"),
    )
    out_specs = (P(("grp", "tp"), "kv"), P(("grp", "kv"), "tp", None, None))
    return jax.shard_map(
        per_device, mesh=mesh, in_specs=in_specs, out_specs=out_specs, check_vma=False
    )
```

profile of v0, /device:TPU:65, one launch (start us, length us, event | category | flops | bytes accessed | tf_op | source)
XLA Modules:
  0.0 336.0 jit_solution(10473639947356605988)
XLA Ops:
  0.6 56.3 %all-gather = bf16[16,12,256]{2,1,0:T(8,128)(2,1)S(1)} all-gather(bf16[1,12,256]{2,1,0:T(8,128)(2,1)} %bitcast.43), channel_id=1, replica_groups=mesh['grp'=2,'kv'=16,'tp'=16] {'tp'}, dimensions={0}, use_global_device_ids=true | all-gather | bytes 104448 | tf_op jit(solution)/shard_map/all_gather | solution.py:51
  57.0 0.1 fusion.3
  57.1 0.2 convert_element_type.186
  57.4 1.0 convolution_convert_fusion.2
  58.3 0.1 concatenate.62
  58.4 0.3 convolution_convert_fusion.3
  58.8 0.5 concatenate.63
  59.3 42.3 %all_to_all.45 = bf16[16,12,1377]{2,1,0:T(8,128)(2,1)S(1)} all-to-all(bf16[16,12,1377]{2,1,0:T(8,128)(2,1)S(1)} %concatenate.63), channel_id=1, replica_groups=mesh['grp'=2,'kv'=16,'tp'=16] {'kv'}, dimensions={0} | all-to-all | bytes 1057536 | tf_op jit(solution)/shard_map/all_to_all | solution.py:19
  101.6 0.1 convert_reduce_fusion.1
  101.7 0.2 fusion.44
  101.9 0.1 fusion.19
  102.1 26.0 %all_to_all.46 = bf16[16,12,688]{2,1,0:T(8,128)(2,1)S(1)} all-to-all(bf16[16,12,688]{2,1,0:T(8,128)(2,1)S(1)} %broadcast_in_dim.6), channel_id=1, replica_groups=mesh['grp'=2,'kv'=16,'tp'=16] {'kv'}, dimensions={0} | all-to-all | bytes 528384 | tf_op jit(solution)/shard_map/all_to_all | solution.py:36
  128.0 0.1 reshape.327
  128.2 0.2 convolution_convert_fusion.6
  128.5 0.7 reshape.328
  129.1 11.7 %all-to-all-start.2 = ((bf16[16,12,256]{2,1,0:T(8,128)(2,1)}), bf16[16,12,256]{2,1,0:T(8,128)(2,1)S(1)}, u32[]{:S(2)}, u32[]{:S(2)}) async-start(bf16[16,12,256]{2,1,0:T(8,128)(2,1)} %reshape.328), calls=%async_computation.2 | async-start | bytes 262144 | tf_op jit(solution)/shard_map/all_to_all | solution.py:19
  140.8 8.9 %all-to-all-done.2 = bf16[16,12,256]{2,1,0:T(8,128)(2,1)S(1)} async-done(((bf16[16,12,256]{2,1,0:T(8,128)(2,1)}), bf16[16,12,256]{2,1,0:T(8,128)(2,1)S(1)}, u32[]{:S(2)}, u32[]{:S(2)}) %all-to-all-start.2) | async-done | bytes 98336 | tf_op jit(solution)/shard_map/all_to_all | solution.py:19
  149.8 14.9 %all-gather.1 = bf16[16,12,256]{2,1,0:T(8,128)(2,1)S(1)} all-gather(bf16[1,12,256]{2,1,0:T(8,128)(2,1)S(1)} %fusion.32), channel_id=1, replica_groups=mesh['grp'=2,'kv'=16,'tp'=16] {'tp'}, dimensions={0}, use_global_device_ids=true | all-gather | bytes 104448 | tf_op jit(solution)/shard_map/all_gather | solution.py:51
  164.7 0.1 fusion.5
  164.8 0.2 convolution_convert_fusion.9
  165.0 0.2 convolution_convert_fusion.8
  165.2 0.2 convolution_convert_fusion.7
  165.4 0.2 convolution_convert_fusion.10
  165.6 0.2 convert_element_type.187
  165.9 0.6 constant_dynamic-update-slice_fusion.4
  166.5 0.6 constant_dynamic-update-slice_fusion.3
  167.2 0.6 constant_dynamic-update-slice_fusion.2
  167.8 0.6 constant_dynamic-update-slice_fusion.1
  168.4 0.6 constant_dynamic-update-slice_fusion
  169.1 5.7 %all-to-all-start.3 = ((bf16[16,12,513]{2,1,0:T(8,128)(2,1)}), bf16[16,12,513]{2,1,0:T(8,128)(2,1)S(1)}, u32[]{:S(2)}, u32[]{:S(2)}) async-start(bf16[16,12,513]{2,1,0:T(8,128)(2,1)} %constant_dynamic-update-slice_fusion), calls=%async_computation.3 | async-start | bytes 655360 | tf_op jit(solution)/shard_map/all_to_all | solution.py:19
  175.0 15.2 %all-to-all-done.3 = bf16[16,12,513]{2,1,0:T(8,128)(2,1)S(1)} async-done(((bf16[16,12,513]{2,1,0:T(8,128)(2,1)}), bf16[16,12,513]{2,1,0:T(8,128)(2,1)S(1)}, u32[]{:S(2)}, u32[]{:S(2)}) %all-to-all-start.3) | async-done | bytes 197024 | tf_op jit(solution)/shard_map/all_to_all | solution.py:19
  190.2 0.1 fusion.41
  190.3 0.1 fusion.38
  190.4 0.1 fusion.28
  190.6 0.8 fusion
  191.4 0.3 fusion.48
  191.7 0.2 fusion.49
  191.9 0.2 multiply_reduce_fusion
  192.1 0.1 multiply_convert_fusion
  192.2 22.9 %all_to_all.47 = bf16[16,12,128]{2,1,0:T(8,128)(2,1)S(1)} all-to-all(bf16[16,12,128]{2,1,0:T(8,128)(2,1)S(1)} %broadcast_in_dim.7), channel_id=1, replica_groups=mesh['grp'=2,'kv'=16,'tp'=16] {'kv'}, dimensions={0} | all-to-all | bytes 98304 | tf_op jit(solution)/shard_map/all_to_all | solution.py:36
  215.2 0.1 convolution_convert_fusion.5
  215.4 15.6 %all_to_all.48 = bf16[16,12,256]{2,1,0:T(8,128)(2,1)S(1)} all-to-all(bf16[16,12,256]{2,1,0:T(8,128)(2,1)S(1)} %reshape.334), channel_id=1, replica_groups=mesh['grp'=2,'kv'=16,'tp'=16] {'tp'}, dimensions={0} | all-to-all | bytes 196608 | tf_op jit(solution)/shard_map/all_to_all | solution.py:19
  231.1 14.9 %all-gather.2 = bf16[16,12,256]{2,1,0:T(8,128)(2,1)S(1)} all-gather(bf16[1,12,256]{2,1,0:T(8,128)(2,1)S(1)} %fusion.33), channel_id=1, replica_groups=mesh['grp'=2,'kv'=16,'tp'=16] {'tp'}, dimensions={0}, use_global_device_ids=true | all-gather | bytes 104448 | tf_op jit(solution)/shard_map/all_gather | solution.py:51
  246.0 0.1 fusion.7
  246.1 0.2 convert_element_type.188
  246.4 0.3 convolution_convert_fusion
  246.8 0.2 copy-done.5
  247.0 0.3 convolution_convert_fusion.1
  247.3 0.5 concatenate.73
  247.8 38.5 %all_to_all.49 = bf16[16,12,1377]{2,1,0:T(8,128)(2,1)S(1)} all-to-all(bf16[16,12,1377]{2,1,0:T(8,128)(2,1)S(1)} %concatenate.73), channel_id=1, replica_groups=mesh['grp'=2,'kv'=16,'tp'=16] {'kv'}, dimensions={0} | all-to-all | bytes 1057536 | tf_op jit(solution)/shard_map/all_to_all | solution.py:19
  286.4 0.1 convert_reduce_fusion
  286.5 0.2 fusion.36
  286.7 0.1 fusion.17
  286.8 0.8 broadcast_in_dim.8
  287.6 8.4 %all-to-all-start.7 = ((bf16[16,12,688]{2,1,0:T(8,128)(2,1)}), bf16[16,12,688]{2,1,0:T(8,128)(2,1)S(1)}, u32[]{:S(2)}, u32[]{:S(2)}) async-start(bf16[16,12,688]{2,1,0:T(8,128)(2,1)} %broadcast_in_dim.8), calls=%async_computation.7 | async-start | bytes 786432 | tf_op jit(solution)/shard_map/all_to_all | solution.py:36
  296.0 0.1 maximum_multiply_fusion
  296.1 17.5 %all-to-all-done.7 = bf16[16,12,688]{2,1,0:T(8,128)(2,1)S(1)} async-done(((bf16[16,12,688]{2,1,0:T(8,128)(2,1)}), bf16[16,12,688]{2,1,0:T(8,128)(2,1)S(1)}, u32[]{:S(2)}, u32[]{:S(2)}) %all-to-all-start.7) | async-done | bytes 264224 | tf_op jit(solution)/shard_map/all_to_all | solution.py:36
  313.6 0.1 reshape.335
  313.7 0.2 convolution_convert_fusion.4
  314.0 0.7 reshape.336
  314.7 11.8 %all-to-all-start.8 = ((bf16[16,12,256]{2,1,0:T(8,128)(2,1)}), bf16[16,12,256]{2,1,0:T(8,128)(2,1)S(1)}, u32[]{:S(2)}, u32[]{:S(2)}) async-start(bf16[16,12,256]{2,1,0:T(8,128)(2,1)} %reshape.336), calls=%async_computation.8 | async-start | bytes 262144 | tf_op jit(solution)/shard_map/all_to_all | solution.py:19
  326.4 1.2 multiply_add_fusion
  327.6 7.7 %all-to-all-done.8 = bf16[16,12,256]{2,1,0:T(8,128)(2,1)S(1)} async-done(((bf16[16,12,256]{2,1,0:T(8,128)(2,1)}), bf16[16,12,256]{2,1,0:T(8,128)(2,1)S(1)}, u32[]{:S(2)}, u32[]{:S(2)}) %all-to-all-start.8) | async-done | bytes 98336 | tf_op jit(solution)/shard_map/all_to_all | solution.py:19
  335.4 0.6 add_convert_fusion
  (61 shorter events, 0.8 us)
Async XLA Ops:
  0.6 56.7 %copy-start = (bf16[256,688]{0,1:T(8,128)(2,1)S(1)}, bf16[256,688]{0,1:T(8,128)(2,1)}, u32[]{:S(2)}) copy-start(bf16[256,688]{0,1:T(8,128)(2,1)} %param.23) | copy-start | bytes 1056772
  57.0 1.4 copy-start.2
  57.0 1.4 copy-start.13
  102.1 26.1 %copy-start.3 = (bf16[688,256]{1,0:T(8,128)(2,1)S(1)}, bf16[688,256]{1,0:T(8,128)(2,1)}, u32[]{:S(2)}) copy-start(bf16[688,256]{1,0:T(8,128)(2,1)} %param.24) | copy-start | bytes 1056772
  128.2 36.6 %copy-start.7 = (bf16[256,128]{1,0:T(8,128)(2,1)S(1)}, bf16[256,128]{1,0:T(8,128)(2,1)}, u32[]{:S(2)}) copy-start(bf16[256,128]{1,0:T(8,128)(2,1)} %param.27) | copy-start | bytes 196612
  128.2 36.6 %copy-start.12 = (f32[256]{0:T(256)S(1)}, f32[256]{0:T(256)}, u32[]{:S(2)}) copy-start(f32[256]{0:T(256)} %param.25) | copy-start | bytes 3076
  128.4 36.6 %copy-start.8 = (bf16[256,128]{1,0:T(8,128)(2,1)S(1)}, bf16[256,128]{1,0:T(8,128)(2,1)}, u32[]{:S(2)}) copy-start(bf16[256,128]{1,0:T(8,128)(2,1)} %param.28) | copy-start | bytes 196612
  129.1 36.1 %copy-start.9 = (bf16[256,128]{1,0:T(8,128)(2,1)S(1)}, bf16[256,128]{1,0:T(8,128)(2,1)}, u32[]{:S(2)}) copy-start(bf16[256,128]{1,0:T(8,128)(2,1)} %param.29) | copy-start | bytes 196612
  129.1 20.6 %all-to-all-start.2 = ((bf16[16,12,256]{2,1,0:T(8,128)(2,1)}), bf16[16,12,256]{2,1,0:T(8,128)(2,1)S(1)}, u32[]{:S(2)}, u32[]{:S(2)}) async-start(bf16[16,12,256]{2,1,0:T(8,128)(2,1)} %reshape.328), calls=%async_computation.2 | async-start | bytes 262144 | tf_op jit(solution)/shard_map/all_to_all | solution.py:19
  140.8 24.6 %copy-start.10 = (bf16[256,128]{1,0:T(8,128)(2,1)S(1)}, bf16[256,128]{1,0:T(8,128)(2,1)}, u32[]{:S(2)}) copy-start(bf16[256,128]{1,0:T(8,128)(2,1)} %param.26) | copy-start | bytes 196612
  165.6 9.3 %copy-start.16 = (s32[12]{0:T(128)S(1)}, s32[12]{0:T(128)}, u32[]{:S(2)}) copy-start(s32[12]{0:T(128)} %param.19) | copy-start | bytes 148
  167.1 23.5 %copy-start.1 = (f32[12,1,128,128]{3,2,1,0:T(8,128)S(1)}, f32[12,1,128,128]{3,2,1,0:T(8,128)}, u32[]{:S(2)}) copy-start(f32[12,1,128,128]{3,2,1,0:T(8,128)} %param.20) | copy-start | bytes 2359300
  169.1 21.1 %all-to-all-start.3 = ((bf16[16,12,513]{2,1,0:T(8,128)(2,1)}), bf16[16,12,513]{2,1,0:T(8,128)(2,1)S(1)}, u32[]{:S(2)}, u32[]{:S(2)}) async-start(bf16[16,12,513]{2,1,0:T(8,128)(2,1)} %constant_dynamic-update-slice_fusion), calls=%async_computation.3 | async-start | bytes 655360 | tf_op jit(solution)/shard_map/all_to_all | solution.py:19
  174.8 17.3 %copy-start.15 = (f32[128]{0:T(128)S(1)}, f32[128]{0:T(128)}, u32[]{:S(2)}) copy-start(f32[128]{0:T(128)} %param.31) | copy-start | bytes 1540
  190.2 25.0 %copy-start.11 = (bf16[128,256]{1,0:T(8,128)(2,1)S(1)}, bf16[128,256]{1,0:T(8,128)(2,1)}, u32[]{:S(2)}) copy-start(bf16[128,256]{1,0:T(8,128)(2,1)} %param.30) | copy-start | bytes 196612
  215.1 31.2 %copy-start.4 = (bf16[256,688]{0,1:T(8,128)(2,1)S(1)}, bf16[256,688]{0,1:T(8,128)(2,1)}, u32[]{:S(2)}) copy-start(bf16[256,688]{0,1:T(8,128)(2,1)} %param.34) | copy-start | bytes 1056772
  215.1 31.3 %copy-start.14 = (f32[256]{0:T(256)S(1)}, f32[256]{0:T(256)}, u32[]{:S(2)}) copy-start(f32[256]{0:T(256)} %param.32) | copy-start | bytes 3076
  246.0 1.0 copy-start.5
  287.6 26.2 %copy-start.6 = (bf16[688,256]{1,0:T(8,128)(2,1)S(1)}, bf16[688,256]{1,0:T(8,128)(2,1)}, u32[]{:S(2)}) copy-start(bf16[688,256]{1,0:T(8,128)(2,1)} %param.35) | copy-start | bytes 1056772
  287.6 26.0 %all-to-all-start.7 = ((bf16[16,12,688]{2,1,0:T(8,128)(2,1)}), bf16[16,12,688]{2,1,0:T(8,128)(2,1)S(1)}, u32[]{:S(2)}, u32[]{:S(2)}) async-start(bf16[16,12,688]{2,1,0:T(8,128)(2,1)} %broadcast_in_dim.8), calls=%async_computation.7 | async-start | bytes 786432 | tf_op jit(solution)/shard_map/all_to_all | solution.py:36
  314.7 20.7 %all-to-all-start.8 = ((bf16[16,12,256]{2,1,0:T(8,128)(2,1)}), bf16[16,12,256]{2,1,0:T(8,128)(2,1)S(1)}, u32[]{:S(2)}, u32[]{:S(2)}) async-start(bf16[16,12,256]{2,1,0:T(8,128)(2,1)} %reshape.336), calls=%async_computation.8 | async-start | bytes 262144 | tf_op jit(solution)/shard_map/all_to_all | solution.py:19
where the time goes:
time: 337 us; the launch traced here: 336 us
  blocking collectives  232 us (69%)
  waiting for transfers between devices  49.3 us (15%)
  starting transfers between devices  37.6 us (11%)
  local copies, waits for them, and re-layouts  8.12 us (2%)
  other arithmetic  4.29 us (1%)
  matrix products  3.82 us (1%)
    all_to_all x3, blocking collectives, sent_and_summed(): lax.all_to_all(parts, axis, split_axis=0, concat_axis=0, tiled=True)  96.5 us
    all_gather x3, blocking collectives, widen_rows(): return lax.all_gather(stream_rows, 'tp', axis=0, tiled=True)  86.1 us
    all_to_all x2, blocking collectives, from_everyone(): lax.all_to_all(jnp.broadcast_to(x[None], (length, *x.shape)), axis, 0, 0,...  48.9 us
    all_to_all x3, waiting for transfers between devices, sent_and_summed(): lax.all_to_all(parts, axis, split_axis=0, concat_axis=0, tiled=True)  31.8 us
    all_to_all x3, starting transfers between devices, sent_and_summed(): lax.all_to_all(parts, axis, split_axis=0, concat_axis=0, tiled=True)  29.2 us
    all_to_all x1, waiting for transfers between devices, from_everyone(): lax.all_to_all(jnp.broadcast_to(x[None], (length, *x.shape)), axis, 0, 0,...  17.5 us
    all_to_all x1, starting transfers between devices, from_everyone(): lax.all_to_all(jnp.broadcast_to(x[None], (length, *x.shape)), axis, 0, 0,...  8.45 us
  transfers between devices with their start and end apart: 4, of which 4 were waited for; matrix products, arithmetic and copies ran while one was open for 0% of the time, Pallas kernels for 0%

commit v1 on v0

--- a/solution.py
+++ b/solution.py
@@ -6,6 +6,11 @@
 D = 4096
 EPS_NORM = 1e-06
 EPS_GROUP = 1e-05
+
+
+def gather_over(x, axis, dim):
+    sent = jnp.stack([x] * lax.axis_size(axis))
+    return jnp.concatenate(lax.all_to_all(sent, axis, 0, 0), axis=dim)
 
 
 def in_blocks(x, dim, length):
@@ -48,7 +53,7 @@
 
 
 def widen_rows(stream_rows):
-    return lax.all_gather(stream_rows, "tp", axis=0, tiled=True)
+    return gather_over(stream_rows, "tp", 0)
 
 
 def prepare(stream, norm_gain):

time: 337 us -> 325 us (0.964)
  blocking collectives: 232 us -> 220 us
    all_gather x3 -> x0, blocking collectives: 86.1 us -> none  [widen_rows(): return lax.all_gather(stream_rows, 'tp', axis=0, tiled=True)]
    all_to_all x0 -> x3, blocking collectives: none -> 75.7 us  [gather_over(): return jnp.concatenate(lax.all_to_all(sent, axis, 0, 0), axis=dim)]
where the time goes in v1:
time: 325 us; the launch traced here: 324 us
  blocking collectives  220 us (68%)
  waiting for transfers between devices  51.5 us (16%)
  starting transfers between devices  34.5 us (11%)
  local copies, waits for them, and re-layouts  9.73 us (3%)
  other arithmetic  4.28 us (1%)
    all_to_all x3, blocking collectives, sent_and_summed(): lax.all_to_all(parts, axis, split_axis=0, concat_axis=0, tiled=True)  96.9 us
    all_to_all x3, blocking collectives, gather_over(): return jnp.concatenate(lax.all_to_all(sent, axis, 0, 0), axis=dim)  75.7 us
    all_to_all x2, blocking collectives, from_everyone(): lax.all_to_all(jnp.broadcast_to(x[None], (length, *x.shape)), axis, 0, 0,...  47 us
    all_to_all x3, waiting for transfers between devices, sent_and_summed(): lax.all_to_all(parts, axis, split_axis=0, concat_axis=0, tiled=True)  34.1 us
    all_to_all x3, starting transfers between devices, sent_and_summed(): lax.all_to_all(parts, axis, split_axis=0, concat_axis=0, tiled=True)  27 us
    all_to_all x1, waiting for transfers between devices, from_everyone(): lax.all_to_all(jnp.broadcast_to(x[None], (length, *x.shape)), axis, 0, 0,...  17.4 us
    all_to_all x1, starting transfers between devices, from_everyone(): lax.all_to_all(jnp.broadcast_to(x[None], (length, *x.shape)), axis, 0, 0,...  7.48 us
  transfers between devices with their start and end apart: 4, of which 4 were waited for; matrix products, arithmetic and copies ran while one was open for 0% of the time, Pallas kernels for 0%

profile of v1, /device:TPU:65, one launch (start us, length us, event | category | flops | bytes accessed | tf_op | source)
XLA Modules:
  0.0 324.1 jit_solution(5338796926630746258)
XLA Ops:
  0.7 0.8 stack.6
  1.4 53.1 %all_to_all.60 = bf16[16,12,256]{2,1,0:T(8,128)(2,1)S(1)} all-to-all(bf16[16,12,256]{2,1,0:T(8,128)(2,1)S(1)} %stack.6), channel_id=1, replica_groups=mesh['grp'=2,'kv'=16,'tp'=16] {'tp'}, dimensions={0} | all-to-all | bytes 196608 | tf_op jit(solution)/shard_map/all_to_all | solution.py:13
  54.5 0.1 multiply_reduce_fusion.2
  54.6 0.2 copy.40
  54.9 0.3 convolution_convert_fusion.2
  55.3 0.6 copy-done.2
  55.8 0.3 convolution_convert_fusion.3
  56.2 0.5 concatenate.63
  56.7 43.3 %all_to_all.61 = bf16[16,12,1377]{2,1,0:T(8,128)(2,1)S(1)} all-to-all(bf16[16,12,1377]{2,1,0:T(8,128)(2,1)S(1)} %concatenate.63), channel_id=1, replica_groups=mesh['grp'=2,'kv'=16,'tp'=16] {'kv'}, dimensions={0} | all-to-all | bytes 1057536 | tf_op jit(solution)/shard_map/all_to_all | solution.py:24
  100.0 0.1 convert_reduce_fusion.1
  100.1 0.2 fusion.28
  100.3 0.1 fusion.5
  100.4 25.6 %all_to_all.62 = bf16[16,12,688]{2,1,0:T(8,128)(2,1)S(1)} all-to-all(bf16[16,12,688]{2,1,0:T(8,128)(2,1)S(1)} %broadcast_in_dim.6), channel_id=1, replica_groups=mesh['grp'=2,'kv'=16,'tp'=16] {'kv'}, dimensions={0} | all-to-all | bytes 528384 | tf_op jit(solution)/shard_map/all_to_all | solution.py:41
  126.1 0.1 reshape.340
  126.2 0.2 convolution_convert_fusion.6
  126.5 0.7 reshape.341
  127.2 10.7 %all-to-all-start.3 = ((bf16[16,12,256]{2,1,0:T(8,128)(2,1)}), bf16[16,12,256]{2,1,0:T(8,128)(2,1)S(1)}, u32[]{:S(2)}, u32[]{:S(2)}) async-start(bf16[16,12,256]{2,1,0:T(8,128)(2,1)} %reshape.341), calls=%async_computation.3 | async-start | bytes 262144 | tf_op jit(solution)/shard_map/all_to_all | solution.py:24
  137.9 9.2 %all-to-all-done.3 = bf16[16,12,256]{2,1,0:T(8,128)(2,1)S(1)} async-done(((bf16[16,12,256]{2,1,0:T(8,128)(2,1)}), bf16[16,12,256]{2,1,0:T(8,128)(2,1)S(1)}, u32[]{:S(2)}, u32[]{:S(2)}) %all-to-all-start.3) | async-done | bytes 98336 | tf_op jit(solution)/shard_map/all_to_all | solution.py:24
  147.2 11.3 %all_to_all.63 = bf16[16,12,256]{2,1,0:T(8,128)(2,1)S(1)} all-to-all(bf16[16,12,256]{2,1,0:T(8,128)(2,1)S(1)} %stack.7), channel_id=1, replica_groups=mesh['grp'=2,'kv'=16,'tp'=16] {'tp'}, dimensions={0} | all-to-all | bytes 196608 | tf_op jit(solution)/shard_map/all_to_all | solution.py:13
  158.6 0.2 convolution_convert_fusion.9
  158.8 0.2 convolution_convert_fusion.8
  159.0 0.2 convolution_convert_fusion.7
  159.1 0.2 convolution_convert_fusion.10
  159.3 0.1 multiply_reduce_fusion.1
  159.5 0.2 copy.41
  159.7 0.6 constant_dynamic-update-slice_fusion.4
  160.3 0.6 constant_dynamic-update-slice_fusion.3
  161.0 0.6 constant_dynamic-update-slice_fusion.2
  161.6 0.6 constant_dynamic-update-slice_fusion.1
  162.2 0.6 constant_dynamic-update-slice_fusion
  162.9 5.7 %all-to-all-start.5 = ((bf16[16,12,513]{2,1,0:T(8,128)(2,1)}), bf16[16,12,513]{2,1,0:T(8,128)(2,1)S(1)}, u32[]{:S(2)}, u32[]{:S(2)}) async-start(bf16[16,12,513]{2,1,0:T(8,128)(2,1)} %constant_dynamic-update-slice_fusion), calls=%async_computation.5 | async-start | bytes 655360 | tf_op jit(solution)/shard_map/all_to_all | solution.py:24
  168.8 16.8 %all-to-all-done.5 = bf16[16,12,513]{2,1,0:T(8,128)(2,1)S(1)} async-done(((bf16[16,12,513]{2,1,0:T(8,128)(2,1)}), bf16[16,12,513]{2,1,0:T(8,128)(2,1)S(1)}, u32[]{:S(2)}, u32[]{:S(2)}) %all-to-all-start.5) | async-done | bytes 197024 | tf_op jit(solution)/shard_map/all_to_all | solution.py:24
  185.6 0.1 fusion.25
  185.8 0.1 fusion.14
  186.0 0.8 fusion
  186.8 0.3 fusion.32
  187.1 0.2 fusion.33
  187.3 0.2 multiply_reduce_fusion.3
  187.5 0.1 multiply_convert_fusion.11
  187.6 21.4 %all_to_all.64 = bf16[16,12,128]{2,1,0:T(8,128)(2,1)S(1)} all-to-all(bf16[16,12,128]{2,1,0:T(8,128)(2,1)S(1)} %broadcast_in_dim.7), channel_id=1, replica_groups=mesh['grp'=2,'kv'=16,'tp'=16] {'kv'}, dimensions={0} | all-to-all | bytes 98304 | tf_op jit(solution)/shard_map/all_to_all | solution.py:41
  209.0 0.1 convolution_convert_fusion.5
  209.2 14.1 %all_to_all.65 = bf16[16,12,256]{2,1,0:T(8,128)(2,1)S(1)} all-to-all(bf16[16,12,256]{2,1,0:T(8,128)(2,1)S(1)} %reshape.348), channel_id=1, replica_groups=mesh['grp'=2,'kv'=16,'tp'=16] {'tp'}, dimensions={0} | all-to-all | bytes 196608 | tf_op jit(solution)/shard_map/all_to_all | solution.py:24
  223.4 11.3 %all_to_all.66 = bf16[16,12,256]{2,1,0:T(8,128)(2,1)S(1)} all-to-all(bf16[16,12,256]{2,1,0:T(8,128)(2,1)S(1)} %stack.8), channel_id=1, replica_groups=mesh['grp'=2,'kv'=16,'tp'=16] {'tp'}, dimensions={0} | all-to-all | bytes 196608 | tf_op jit(solution)/shard_map/all_to_all | solution.py:13
  234.7 0.1 multiply_reduce_fusion
  234.8 0.2 copy.46
  235.1 0.3 convolution_convert_fusion
  235.5 0.6 copy-done.5
  236.0 0.3 convolution_convert_fusion.1
  236.4 0.5 concatenate.73
  236.9 39.5 %all_to_all.67 = bf16[16,12,1377]{2,1,0:T(8,128)(2,1)S(1)} all-to-all(bf16[16,12,1377]{2,1,0:T(8,128)(2,1)S(1)} %concatenate.73), channel_id=1, replica_groups=mesh['grp'=2,'kv'=16,'tp'=16] {'kv'}, dimensions={0} | all-to-all | bytes 1057536 | tf_op jit(solution)/shard_map/all_to_all | solution.py:24
  276.4 0.1 convert_reduce_fusion
  276.6 0.2 fusion.20
  276.7 0.1 fusion.3
  276.9 0.8 broadcast_in_dim.8
  277.6 7.5 %all-to-all-start.10 = ((bf16[16,12,688]{2,1,0:T(8,128)(2,1)}), bf16[16,12,688]{2,1,0:T(8,128)(2,1)S(1)}, u32[]{:S(2)}, u32[]{:S(2)}) async-start(bf16[16,12,688]{2,1,0:T(8,128)(2,1)} %broadcast_in_dim.8), calls=%async_computation.10 | async-start | bytes 786432 | tf_op jit(solution)/shard_map/all_to_all | solution.py:41
  285.1 0.1 maximum_multiply_fusion
  285.2 17.4 %all-to-all-done.10 = bf16[16,12,688]{2,1,0:T(8,128)(2,1)S(1)} async-done(((bf16[16,12,688]{2,1,0:T(8,128)(2,1)}), bf16[16,12,688]{2,1,0:T(8,128)(2,1)S(1)}, u32[]{:S(2)}, u32[]{:S(2)}) %all-to-all-start.10) | async-done | bytes 264224 | tf_op jit(solution)/shard_map/all_to_all | solution.py:41
  302.6 0.1 reshape.350
  302.7 0.2 convolution_convert_fusion.4
  303.0 0.7 reshape.351
  303.6 10.6 %all-to-all-start.11 = ((bf16[16,12,256]{2,1,0:T(8,128)(2,1)}), bf16[16,12,256]{2,1,0:T(8,128)(2,1)S(1)}, u32[]{:S(2)}, u32[]{:S(2)}) async-start(bf16[16,12,256]{2,1,0:T(8,128)(2,1)} %reshape.351), calls=%async_computation.11 | async-start | bytes 262144 | tf_op jit(solution)/shard_map/all_to_all | solution.py:24
  314.2 1.1 multiply_add_fusion
  315.4 8.1 %all-to-all-done.11 = bf16[16,12,256]{2,1,0:T(8,128)(2,1)S(1)} async-done(((bf16[16,12,256]{2,1,0:T(8,128)(2,1)}), bf16[16,12,256]{2,1,0:T(8,128)(2,1)S(1)}, u32[]{:S(2)}, u32[]{:S(2)}) %all-to-all-start.11) | async-done | bytes 98336 | tf_op jit(solution)/shard_map/all_to_all | solution.py:24
  323.5 0.6 add_convert_fusion
  (64 shorter events, 1.0 us)
Async XLA Ops:
  0.6 54.3 %copy-start = (bf16[256,688]{0,1:T(8,128)(2,1)S(1)}, bf16[256,688]{0,1:T(8,128)(2,1)}, u32[]{:S(2)}) copy-start(bf16[256,688]{0,1:T(8,128)(2,1)} %param.23) | copy-start | bytes 1056772
  0.6 54.3 %copy-start.13 = (f32[256]{0:T(256)S(1)}, f32[256]{0:T(256)}, u32[]{:S(2)}) copy-start(f32[256]{0:T(256)} %param.21) | copy-start | bytes 3076
  54.9 1.0 copy-start.2
  100.4 25.8 %copy-start.3 = (bf16[688,256]{1,0:T(8,128)(2,1)S(1)}, bf16[688,256]{1,0:T(8,128)(2,1)}, u32[]{:S(2)}) copy-start(bf16[688,256]{1,0:T(8,128)(2,1)} %param.24) | copy-start | bytes 1056772
  126.4 32.1 %copy-start.7 = (bf16[256,128]{1,0:T(8,128)(2,1)S(1)}, bf16[256,128]{1,0:T(8,128)(2,1)}, u32[]{:S(2)}) copy-start(bf16[256,128]{1,0:T(8,128)(2,1)} %param.27) | copy-start | bytes 196612
  126.4 32.1 %copy-start.12 = (f32[256]{0:T(256)S(1)}, f32[256]{0:T(256)}, u32[]{:S(2)}) copy-start(f32[256]{0:T(256)} %param.25) | copy-start | bytes 3076
  126.5 32.3 %copy-start.8 = (bf16[256,128]{1,0:T(8,128)(2,1)S(1)}, bf16[256,128]{1,0:T(8,128)(2,1)}, u32[]{:S(2)}) copy-start(bf16[256,128]{1,0:T(8,128)(2,1)} %param.28) | copy-start | bytes 196612
  127.2 19.9 %all-to-all-start.3 = ((bf16[16,12,256]{2,1,0:T(8,128)(2,1)}), bf16[16,12,256]{2,1,0:T(8,128)(2,1)S(1)}, u32[]{:S(2)}, u32[]{:S(2)}) async-start(bf16[16,12,256]{2,1,0:T(8,128)(2,1)} %reshape.341), calls=%async_computation.3 | async-start | bytes 262144 | tf_op jit(solution)/shard_map/all_to_all | solution.py:24
  137.8 21.1 %copy-start.9 = (bf16[256,128]{1,0:T(8,128)(2,1)S(1)}, bf16[256,128]{1,0:T(8,128)(2,1)}, u32[]{:S(2)}) copy-start(bf16[256,128]{1,0:T(8,128)(2,1)} %param.29) | copy-start | bytes 196612
  147.2 12.0 %copy-start.10 = (bf16[256,128]{1,0:T(8,128)(2,1)S(1)}, bf16[256,128]{1,0:T(8,128)(2,1)}, u32[]{:S(2)}) copy-start(bf16[256,128]{1,0:T(8,128)(2,1)} %param.26) | copy-start | bytes 196612
  159.3 9.4 %copy-start.16 = (s32[12]{0:T(128)S(1)}, s32[12]{0:T(128)}, u32[]{:S(2)}) copy-start(s32[12]{0:T(128)} %param.19) | copy-start | bytes 148
  161.0 25.0 %copy-start.1 = (f32[12,1,128,128]{3,2,1,0:T(8,128)S(1)}, f32[12,1,128,128]{3,2,1,0:T(8,128)}, u32[]{:S(2)}) copy-start(f32[12,1,128,128]{3,2,1,0:T(8,128)} %param.20) | copy-start | bytes 2359300
  162.9 22.7 %all-to-all-start.5 = ((bf16[16,12,513]{2,1,0:T(8,128)(2,1)}), bf16[16,12,513]{2,1,0:T(8,128)(2,1)S(1)}, u32[]{:S(2)}, u32[]{:S(2)}) async-start(bf16[16,12,513]{2,1,0:T(8,128)(2,1)} %constant_dynamic-update-slice_fusion), calls=%async_computation.5 | async-start | bytes 655360 | tf_op jit(solution)/shard_map/all_to_all | solution.py:24
  168.6 18.9 %copy-start.15 = (f32[128]{0:T(128)S(1)}, f32[128]{0:T(128)}, u32[]{:S(2)}) copy-start(f32[128]{0:T(128)} %param.31) | copy-start | bytes 1540
  185.6 23.4 %copy-start.11 = (bf16[128,256]{1,0:T(8,128)(2,1)S(1)}, bf16[128,256]{1,0:T(8,128)(2,1)}, u32[]{:S(2)}) copy-start(bf16[128,256]{1,0:T(8,128)(2,1)} %param.30) | copy-start | bytes 196612
  209.2 25.9 %copy-start.4 = (bf16[256,688]{0,1:T(8,128)(2,1)S(1)}, bf16[256,688]{0,1:T(8,128)(2,1)}, u32[]{:S(2)}) copy-start(bf16[256,688]{0,1:T(8,128)(2,1)} %param.34) | copy-start | bytes 1056772
  209.2 25.9 %copy-start.14 = (f32[256]{0:T(256)S(1)}, f32[256]{0:T(256)}, u32[]{:S(2)}) copy-start(f32[256]{0:T(256)} %param.32) | copy-start | bytes 3076
  235.0 1.0 copy-start.5
  277.6 25.1 %copy-start.6 = (bf16[688,256]{1,0:T(8,128)(2,1)S(1)}, bf16[688,256]{1,0:T(8,128)(2,1)}, u32[]{:S(2)}) copy-start(bf16[688,256]{1,0:T(8,128)(2,1)} %param.35) | copy-start | bytes 1056772
  277.6 25.0 %all-to-all-start.10 = ((bf16[16,12,688]{2,1,0:T(8,128)(2,1)}), bf16[16,12,688]{2,1,0:T(8,128)(2,1)S(1)}, u32[]{:S(2)}, u32[]{:S(2)}) async-start(bf16[16,12,688]{2,1,0:T(8,128)(2,1)} %broadcast_in_dim.8), calls=%async_computation.10 | async-start | bytes 786432 | tf_op jit(solution)/shard_map/all_to_all | solution.py:41
  303.6 19.8 %all-to-all-start.11 = ((bf16[16,12,256]{2,1,0:T(8,128)(2,1)}), bf16[16,12,256]{2,1,0:T(8,128)(2,1)S(1)}, u32[]{:S(2)}, u32[]{:S(2)}) async-start(bf16[16,12,256]{2,1,0:T(8,128)(2,1)} %reshape.351), calls=%async_computation.11 | async-start | bytes 262144 | tf_op jit(solution)/shard_map/all_to_all | solution.py:24
